TPU v7x, 32 devices: a whole 2x2x4 slice. The times are simulated.
32 devices in a mesh: sp: 4 (over y, x), dp: 8 (over z, core).
Axes of the slice: x: 2, y: 2, z: 4, core: 2. Of those that a mesh axis runs over, the one named last changes fastest.
Arguments:
- tokens: bfloat16 [8, 768, 4096], P('dp', 'sp'), may hold values from -30 to 30
- query_weight: bfloat16 [4096, 512], P('dp', 'sp'), may hold values from -0.09375 to 0.09375
- key_weight: bfloat16 [4096, 512], P('dp', 'sp'), may hold values from -0.09375 to 0.09375
- value_weight: bfloat16 [4096, 512], P('dp', 'sp'), may hold values from -0.09375 to 0.09375
- cum_gate: float32 [8, 4, 768], P('dp', 'sp'), may hold values from -3072 to 0, as said below
Outputs:
- attended: bfloat16 [8, 768, 512], P('dp', 'sp')
Inputs may be any that keep to these rules, and one draw needn't show every extreme that they name: `cum_gate`: never rising along positions; the first position holds one step's log gate.
All inputs are finite; a program needn't handle non-finite values.
Results may differ from a plain program's by a relative error of at most 0.0076.
The roundings to bfloat16 on the way count: a program that leaves them out, or rounds other values in their place, can miss the bound.
Values may be sent and summed in bfloat16 or wider, within the bound.
A program may use at most 128 MiB of HBM per device.

v0:
```python
import functools
import math

import jax
import jax.numpy as jnp
from jax import lax
from jax.experimental import pallas as pl
from jax.experimental.pallas import tpu as pltpu
from jax.sharding import PartitionSpec as P

MESH = pl.DeviceIdType.MESH
block_rows = 256


def kernel(
    nx, ny, nz, cores,
    tok_hbm, wq_hbm, wk_hbm, wv_hbm, gate_ref, out_ref,
    xbuf, wbuf, acc, qkv, qout, gcol, attn, obuf,
    lsem, tsem, xsend, xrecv, wrecv, upsem, downsem, upq, downq, psem, pq, ysem, yq,
    qsend, qrecv, osend, orecv,
):
    tok, depth = tok_hbm.shape
    rows, head = wq_hbm.shape
    early = rows // 16
    chunk = cores * rows
    group = nx * tok
    length = ny * group
    s, d = lax.axis_index("sp"), lax.axis_index("dp")
    y, x = s // nx, s % nx
    z, c = d // cores, d % cores

    def piece(zb):
        return tok_hbm.at[:, pl.ds(pl.multiple_of(zb * chunk, chunk), chunk)]

    loads = [
        pltpu.make_async_copy(ref, wbuf.at[y, d, :, pl.ds(i * head, head)], lsem.at[i])
        for i, ref in enumerate((wq_hbm, wk_hbm, wv_hbm))
    ]
    own_loads = [
        pltpu.make_async_copy(piece(zb), xbuf.at[x, zb], tsem.at[zb]) for zb in range(nz)
    ]
    for load in loads + own_loads:
        load.start()

    barrier = pltpu.get_barrier_semaphore()
    for k in range(1, nx * ny):
        pl.semaphore_signal(
            barrier, inc=1, device_id={"sp": (s + k) % (nx * ny)}, device_id_type=MESH
        )
    for k in range(1, nz):
        pl.semaphore_signal(
            barrier, inc=1, device_id={"dp": ((z + k) % nz) * cores + c}, device_id_type=MESH
        )
    if cores > 1:
        pl.semaphore_signal(
            barrier, inc=1, device_id={"dp": z * cores + 1 - c}, device_id_type=MESH
        )
    pl.semaphore_wait(barrier, nx * ny - 1 + nz - 1 + cores - 1)

    def step(t, act):
        if t == 0:
            act(z)
            return
        pl.when(z - t >= 0)(lambda: act(z - t))
        pl.when(z + t < nz)(lambda: act(z + t))

    def send_tokens(j, zb):
        return pltpu.make_async_remote_copy(
            src_ref=piece(zb), dst_ref=xbuf.at[x, zb],
            send_sem=xsend.at[j - 1, zb], recv_sem=xrecv.at[x, zb],
            device_id={"sp": y * nx + (x + j) % nx}, device_id_type=MESH,
        )

    def view(h, at, part):
        if part == 0:
            return wbuf.at[h, at]
        if part == 1:
            return wbuf.at[h, at, pl.ds(0, early)]
        return wbuf.at[h, at, pl.ds(early, rows - early)]

    def send_block(h, zb, part, sem, device):
        at = zb * cores + c
        return pltpu.make_async_remote_copy(
            src_ref=view(h, at, part), dst_ref=view(h, at, part),
            send_sem=sem, recv_sem=wrecv.at[int(part == 1), h, at],
            device_id=device, device_id_type=MESH,
        )

    above = {"dp": jnp.minimum(z + 1, nz - 1) * cores + c}
    below = {"dp": jnp.maximum(z - 1, 0) * cores + c}
    beside = {"dp": z * cores + 1 - c}

    def aside(k):
        return {"sp": ((y + k) % ny) * nx + x}

    def up(zb):
        return send_block(y, zb, 0, upsem.at[zb], above)

    def down(zb):
        return send_block(y, zb, 0, downsem.at[zb], below)

    def up_early(h, zb):
        return send_block(h, zb, 1, upq.at[h, zb], above)

    def down_early(h, zb):
        return send_block(h, zb, 1, downq.at[h, zb], below)

    def across(h, zb, part):
        return send_block(h, zb, part, (pq if part == 1 else psem).at[h, zb], beside)

    def side_early(k):
        return send_block(y, z, 1, yq.at[k - 1], aside(k))

    def side_late(k, zb):
        return send_block(y, zb, 2, ysem.at[k - 1, zb], aside(k))

    def arrived(h, at, part):
        pltpu.make_async_remote_copy(
            src_ref=view(h, at, part), dst_ref=view(h, at, part),
            send_sem=lsem.at[0], recv_sem=wrecv.at[int(part == 1), h, at],
            device_id={"sp": (s + 1) % (nx * ny)}, device_id_type=MESH,
        ).wait_recv()

    others = [(y + k) % ny for k in range(1, ny)]

    for load in loads:
        load.wait()

    def spread(zb):
        for k in range(1, ny):
            side_late(k, zb).start()
        if cores > 1:
            across(y, zb, 0).start()

    for k in range(1, ny):
        side_early(k).start()
    pl.when(z < nz - 1)(lambda: up(z).start())
    pl.when(z > 0)(lambda: down(z).start())
    for j in range(1, nx):
        send_tokens(j, z).start()
    spread(z)
    for t in range(1, nz):
        for j in range(1, nx):
            step(t, lambda zb, j=j: send_tokens(j, zb).start())

    for start in range(0, length, 128):
        row = gate_ref[:, start : start + 128]
        gcol[start : start + 128, :] = jnp.broadcast_to(row, (128, 128)).T
    acc[...] = jnp.zeros_like(acc)

    def relay(t):
        def from_below(zb):
            arrived(y, zb * cores + c, 0)
            pl.when(z < nz - 1)(lambda: up(zb).start())
            spread(zb)

        def from_above(zb):
            arrived(y, zb * cores + c, 0)
            pl.when(z > 0)(lambda: down(zb).start())
            spread(zb)

        def hand_on(zb, upward, downward):
            for h in others:
                arrived(h, zb * cores + c, 1)
                if upward:
                    pl.when(z < nz - 1)(lambda h=h: up_early(h, zb).start())
                if downward:
                    pl.when(z > 0)(lambda h=h: down_early(h, zb).start())
                if cores > 1:
                    across(h, zb, 1).start()

        if t == 0:
            hand_on(z, True, True)
            return
        pl.when(z - t >= 0)(lambda: from_below(z - t))
        pl.when(z + t < nz)(lambda: from_above(z + t))
        pl.when(z - t >= 0)(lambda: hand_on(z - t, True, False))
        pl.when(z + t < nz)(lambda: hand_on(z + t, False, True))

    def from_side(zb):
        for h in others:
            arrived(h, zb * cores + c, 2)
            if cores > 1:
                across(h, zb, 2).start()

    def add(zb, i):
        for h in others + [y]:
            weights = wbuf[h, pl.ds(zb * cores, cores)].reshape(chunk, 3 * head)
            acc[h, i] += jnp.dot(xbuf[i, zb], weights, preferred_element_type=jnp.float32)

    def add_own(zb):
        if cores > 1:
            at = zb * cores + 1 - c
            arrived(y, at, 0)
            for h in others:
                arrived(h, at, 1)
                arrived(h, at, 2)
        pltpu.make_async_copy(piece(zb), xbuf.at[x, zb], tsem.at[zb]).wait()
        add(zb, x)

    def add_other(zb):
        for j in range(1, nx):
            i = (x + j) % nx
            pltpu.make_async_remote_copy(
                src_ref=piece(zb), dst_ref=xbuf.at[i, zb],
                send_sem=xsend.at[j - 1, zb], recv_sem=xrecv.at[i, zb],
                device_id={"sp": (s + 1) % (nx * ny)}, device_id_type=MESH,
            ).wait_recv()
            add(zb, i)

    def own_rows(i):
        return pl.ds(pl.multiple_of(y * group + i * tok, tok), tok)

    def send_qkv(k, i):
        return pltpu.make_async_remote_copy(
            src_ref=qout.at[k - 1, i], dst_ref=qkv.at[own_rows(i)],
            send_sem=qsend.at[k - 1, i], recv_sem=qrecv.at[y, i],
            device_id=aside(k), device_id_type=MESH,
        )

    def swap(i):
        for k in range(1, ny):
            qout[k - 1, i] = acc[others[k - 1], i].astype(jnp.bfloat16)
            send_qkv(k, i).start()

    relay(0)
    for t in range(nz):
        if t + 1 < nz:
            relay(t + 1)
        step(t, from_side)
        step(t, add_own)
        if t == nz - 1:
            swap(x)
        step(t, add_other)
    for j in range(1, nx):
        swap((x + j) % nx)
    for i in range(nx):
        qkv[own_rows(i), :] = acc[y, i].astype(jnp.bfloat16)
    for k in range(1, ny):
        other = (y + k) % ny
        for i in range(nx):
            taken = pl.ds(pl.multiple_of(other * group + i * tok, tok), tok)
            pltpu.make_async_remote_copy(
                src_ref=qout.at[k - 1, i], dst_ref=qkv.at[taken],
                send_sem=qsend.at[k - 1, i], recv_sem=qrecv.at[other, i],
                device_id={"sp": other * nx + x}, device_id_type=MESH,
            ).wait_recv()

    def send_out(to):
        return pltpu.make_async_remote_copy(
            src_ref=attn.at[pl.ds(to * tok, tok)],
            dst_ref=obuf.at[:, pl.ds(pl.multiple_of(s * head, head), head)],
            send_sem=osend.at[to], recv_sem=orecv.at[s],
            device_id={"sp": to}, device_id_type=MESH,
        )

    scale = head ** (-0.5)
    sent = 0
    for start in range(0, length, block_rows):
        finish = min(start + block_rows, length)
        scores = (
            lax.dot_general(
                qkv[start:finish, :head], qkv[:finish, head : 2 * head],
                (((1,), (1,)), ((), ())), preferred_element_type=jnp.float32,
            )
            * scale
        )
        scores = scores + gcol[start:finish, :1] - gate_ref[:, :finish]
        rows_at = start + lax.broadcasted_iota(jnp.int32, scores.shape, 0)
        cols_at = lax.broadcasted_iota(jnp.int32, scores.shape, 1)
        scores = jnp.where(cols_at <= rows_at, scores, -1e30)
        top = jnp.max(scores, axis=1, keepdims=True)
        weights = jnp.exp(scores - top)
        total = jnp.sum(weights, axis=1, keepdims=True)
        summed = jnp.dot(
            weights.astype(jnp.bfloat16), qkv[:finish, 2 * head :],
            preferred_element_type=jnp.float32,
        )
        attn[start:finish, :] = (summed / total).astype(jnp.bfloat16)
        while (sent + 1) * tok <= finish:

            @pl.when(s != sent)
            def _(to=sent):
                send_out(to).start()

            @pl.when(s == sent)
            def _(to=sent):
                obuf[:, pl.ds(pl.multiple_of(s * head, head), head)] = attn[
                    to * tok : (to + 1) * tok, :
                ]

            sent += 1

    for k in range(1, nx * ny):
        source = (s + k) % (nx * ny)
        pltpu.make_async_remote_copy(
            src_ref=attn.at[pl.ds(0, tok)],
            dst_ref=obuf.at[:, pl.ds(pl.multiple_of(source * head, head), head)],
            send_sem=osend.at[source], recv_sem=orecv.at[source],
            device_id={"sp": source}, device_id_type=MESH,
        ).wait_recv()
    last = pltpu.make_async_copy(obuf, out_ref, lsem.at[0])
    last.start()

    for zb in range(nz):
        for j in range(1, nx):
            send_tokens(j, zb).wait_send()
        upward = (z < nz - 1) & (zb <= z)
        downward = (z > 0) & (zb >= z)
        pl.when(upward)(lambda zb=zb: up(zb).wait_send())
        pl.when(downward)(lambda zb=zb: down(zb).wait_send())
        for h in others:
            pl.when(upward)(lambda h=h, zb=zb: up_early(h, zb).wait_send())
            pl.when(downward)(lambda h=h, zb=zb: down_early(h, zb).wait_send())
            if cores > 1:
                across(h, zb, 1).wait_send()
                across(h, zb, 2).wait_send()
        if cores > 1:
            across(y, zb, 0).wait_send()
        for k in range(1, ny):
            side_late(k, zb).wait_send()
    for k in range(1, ny):
        side_early(k).wait_send()
    for k in range(1, ny):
        for i in range(nx):
            send_qkv(k, i).wait_send()
    for to in range(nx * ny):
        pl.when(s != to)(lambda to=to: send_out(to).wait_send())
    last.wait()


def body(sp, dp, tokens, query_weight, key_weight, value_weight, cum_gate):
    nx = max(n for n in range(1, math.isqrt(sp) + 1) if sp % n == 0)
    ny = sp // nx
    cores = 2 if dp % 2 == 0 else 1
    nz = dp // cores
    tok, depth = tokens.shape[1:]
    rows, head = query_weight.shape
    length = sp * tok
    dma = pltpu.SemaphoreType.DMA
    anywhere = pl.BlockSpec(memory_space=pl.ANY)
    vmem = pl.BlockSpec(memory_space=pltpu.VMEM)
    out = pl.pallas_call(
        functools.partial(kernel, nx, ny, nz, cores),
        out_shape=jax.ShapeDtypeStruct((tok, sp * head), jnp.bfloat16),
        in_specs=[anywhere] * 4 + [vmem],
        out_specs=anywhere,
        scratch_shapes=[
            pltpu.VMEM((nx, nz, tok, cores * rows), jnp.bfloat16),
            pltpu.VMEM((ny, dp, rows, 3 * head), jnp.bfloat16),
            pltpu.VMEM((ny, nx, tok, 3 * head), jnp.float32),
            pltpu.VMEM((length, 3 * head), jnp.bfloat16),
            pltpu.VMEM((ny - 1, nx, tok, 3 * head), jnp.bfloat16),
            pltpu.VMEM((length, 128), jnp.float32),
            pltpu.VMEM((length, head), jnp.bfloat16),
            pltpu.VMEM((tok, sp * head), jnp.bfloat16),
            dma((3,)),
            dma((nz,)),
            dma((nx - 1, nz)),
            dma((nx, nz)),
            dma((2, ny, dp)),
            dma((nz,)),
            dma((nz,)),
            dma((ny, nz)),
            dma((ny, nz)),
            dma((ny, nz)),
            dma((ny, nz)),
            dma((ny - 1, nz)),
            dma((ny - 1,)),
            dma((ny - 1, nx)),
            dma((ny, nx)),
            dma((sp,)),
            dma((sp,)),
        ],
        compiler_params=pltpu.CompilerParams(
            collective_id=0, has_side_effects=True, vmem_limit_bytes=60 * 1024 * 1024
        ),
    )(tokens[0], query_weight, key_weight, value_weight, cum_gate[0])
    return out[None]


def solution(mesh):
    in_specs = (
        P("dp", "sp", None),
        P("dp", "sp"),
        P("dp", "sp"),
        P("dp", "sp"),
        P("dp", "sp", None),
    )
    out_specs = P("dp", "sp", None)
    return jax.shard_map(
        functools.partial(body, mesh.shape["sp"], mesh.shape["dp"]),
        mesh=mesh, in_specs=in_specs, out_specs=out_specs, check_vma=False,
    )
```

profile of v0, /device:TPU:0, one launch (start us, length us, event | category | flops | bytes accessed | tf_op | source)
XLA Modules:
  0.0 58.9 jit_solution(15668599234004367822)
XLA Ops:
  0.0 57.2 %shard_map.55 = bf16[192,512]{1,0:T(8,128)(2,1)} custom-call(bf16[192,4096]{1,0:T(8,128)(2,1)} %bitcast.3, bf16[512,128]{1,0:T(8,128)(2,1)} %wq_hbm.1, bf16[512,128]{1,0:T(8,128)(2,1)} %wk_hbm.1, bf16[512,128]{1,0:T(8,128)(2,1)} %wv_hbm.1, f32[1,768]{1,0:T(1,128)} %bitcast.5), custom_call_target="tpu_custom_call" | custom-call | tf_op jit(solution)/shard_map/pallas_call | solution.py:343
  57.2 1.6 %copy.7 = bf16[1,192,512]{2,1,0:T(8,128)(2,1)} copy(bf16[1,192,512]{2,1,0:T(8,128)(2,1)} %bitcast.4) | data formatting | bytes 393216
where the time goes:
time: 59 us; the launch traced here: 58.9 us
  Pallas kernels  57.2 us (97%)
  local copies, waits for them, and re-layouts  1.62 us (3%)
    pallas_call x1, Pallas kernels, body(): pl.pallas_call(functools.partial(kernel, nx, ny, nz, cores), out_shape=ja...  57.2 us
    unnamed x1, local copies, waits for them, and re-layouts  1.62 us

commit v1 on v0

v1 whole, which is shorter than its diff:
```python
import functools
import math

import jax
import jax.numpy as jnp
from jax import lax
from jax.experimental import pallas as pl
from jax.experimental.pallas import tpu as pltpu
from jax.sharding import PartitionSpec as P

MESH = pl.DeviceIdType.MESH
block_rows = 256


def kernel(
    nx, ny, nz, cores, split, sub, early,
    tok_hbm, wq_hbm, wk_hbm, wv_hbm, gate_ref, out_ref,
    xbuf, wbuf, acc, qkv, qout, gcol, attn, obuf,
    lsem, tsem, xsend, xrecv, wrecv, precv, upsem, downsem, sideq, sidesem, psem,
    qsend, qrecv, osend, orecv,
):
    tok, depth = tok_hbm.shape
    rows, head = wq_hbm.shape
    pieces = rows // sub
    chunk = cores * rows
    group = nx * tok
    length = ny * group
    s, d = lax.axis_index("sp"), lax.axis_index("dp")
    y, x = s // nx, s % nx
    z, c = d // cores, d % cores
    others = [(y + k) % ny for k in range(1, ny)]
    early_rows = pl.ds(0, early * sub)
    late_rows = pl.ds(early * sub, rows - early * sub)
    parts = (pl.ds(0, split), pl.ds(split, tok - split))

    def columns(zb):
        return pl.ds(pl.multiple_of(zb * chunk, chunk), chunk)

    low = jnp.minimum(z, nz - 1 - z)

    def nearest(k):
        if k == 0:
            return z
        near = z - (k + 1) // 2 if k % 2 else z + k // 2
        far = jnp.where(z < nz - 1 - z, z + k - low, z - k + low)
        return jnp.where(k <= 2 * low, near, far)

    loads = [
        pltpu.make_async_copy(ref, wbuf.at[y, d, :, pl.ds(i * head, head)], lsem.at[i])
        for i, ref in enumerate((wq_hbm, wk_hbm, wv_hbm))
    ]
    own_load = pltpu.make_async_copy(tok_hbm, xbuf.at[x], tsem)
    for load in loads:
        load.start()
    own_load.start()

    barrier = pltpu.get_barrier_semaphore()
    for k in range(1, nx * ny):
        pl.semaphore_signal(
            barrier, inc=1, device_id={"sp": (s + k) % (nx * ny)}, device_id_type=MESH
        )
    above = {"dp": jnp.minimum(z + 1, nz - 1) * cores + c}
    below = {"dp": jnp.maximum(z - 1, 0) * cores + c}
    beside = {"dp": z * cores + 1 - c}

    @pl.when(z < nz - 1)
    def _():
        pl.semaphore_signal(barrier, inc=1, device_id=above, device_id_type=MESH)

    @pl.when(z > 0)
    def _():
        pl.semaphore_signal(barrier, inc=1, device_id=below, device_id_type=MESH)

    if cores > 1:
        pl.semaphore_signal(barrier, inc=1, device_id=beside, device_id_type=MESH)
    inner = (z > 0) & (z < nz - 1)
    ends = jnp.where(inner, 2, 1) if nz > 1 else 0
    pl.semaphore_wait(barrier, nx * ny - 1 + cores - 1 + ends)

    def aside(k):
        return {"sp": ((y + k) % ny) * nx + x}

    def send_tokens(j, zb, g):
        return pltpu.make_async_remote_copy(
            src_ref=tok_hbm.at[parts[g], columns(zb)],
            dst_ref=xbuf.at[x, parts[g], columns(zb)],
            send_sem=xsend.at[j - 1, zb, g], recv_sem=xrecv.at[x, zb, g],
            device_id={"sp": y * nx + (x + j) % nx}, device_id_type=MESH,
        )

    def tokens_here(zb, g):
        for j in range(1, nx):
            i = (x + j) % nx
            pltpu.make_async_remote_copy(
                src_ref=tok_hbm.at[parts[g], columns(zb)],
                dst_ref=xbuf.at[i, parts[g], columns(zb)],
                send_sem=xsend.at[j - 1, zb, g], recv_sem=xrecv.at[i, zb, g],
                device_id={"sp": y * nx + i}, device_id_type=MESH,
            ).wait_recv()

    def piece(p):
        return pl.ds(pl.multiple_of(p * sub, sub), sub)

    def copy_block(h, at, part, send_sem, recv_sem, device):
        ref = wbuf.at[h, at, part]
        return pltpu.make_async_remote_copy(
            src_ref=ref, dst_ref=ref, send_sem=send_sem, recv_sem=recv_sem,
            device_id=device, device_id_type=MESH,
        )

    def up(h, zb, part, p):
        return copy_block(h, zb * cores + c, part, upsem.at[h, zb], wrecv.at[h, zb, p], above)

    def down(h, zb, part, p):
        return copy_block(h, zb * cores + c, part, downsem.at[h, zb], wrecv.at[h, zb, p], below)

    def side_early(k, p):
        return copy_block(y, d, piece(p), sideq.at[k - 1], wrecv.at[y, z, p], aside(k))

    def side(k, zb, part):
        return copy_block(
            y, zb * cores + c, part, sidesem.at[k - 1, zb], wrecv.at[y, zb, early], aside(k)
        )

    def pair(h, zb, which, core):
        part = early_rows if which else late_rows
        return copy_block(
            h, zb * cores + core, part, psem.at[h, zb, which], precv.at[h, zb, which], beside
        )

    def arrived(h, zb, part, p):
        copy_block(
            h, zb * cores + c, part, lsem.at[0], wrecv.at[h, zb, p], aside(1)
        ).wait_recv()

    def share(h, zb, which):
        if cores > 1:
            pair(h, zb, which, c).start()

    def shared(h, zb):
        if cores > 1:
            for which in range(2):
                pair(h, zb, which, 1 - c).wait_recv()

    def both_ways(h, zb, p):
        pl.when(z < nz - 1)(lambda: up(h, zb, piece(p), p).start())
        pl.when(z > 0)(lambda: down(h, zb, piece(p), p).start())

    def pass_on(h, zb, p, rising):
        if rising:
            pl.when(z < nz - 1)(lambda: up(h, zb, piece(p), p).start())
        else:
            pl.when(z > 0)(lambda: down(h, zb, piece(p), p).start())

    def each(t, act):
        pl.when(z - t >= 0)(lambda: act(z - t, True))
        pl.when(z + t < nz)(lambda: act(z + t, False))

    def loop(first, last, act):
        def step(p, carry):
            act(p)
            return carry

        lax.fori_loop(first, last, step, 0)

    def relay_own(t, crosses):
        def take(p):
            def one(zb, rising):
                arrived(y, zb, piece(p), p)
                pass_on(y, zb, p, rising)
                if crosses:
                    for k in range(1, ny):
                        side(k, zb, piece(p)).start()

            each(t, one)

        loop(early if crosses else 0, pieces if crosses else early, take)
        each(t, lambda zb, rising: share(y, zb, 0 if crosses else 1))

    def relay_other(t):
        def take(p):
            for h in others:
                if t == 0:
                    arrived(h, z, piece(p), p)
                    both_ways(h, z, p)
                    continue

                def one(zb, rising, h=h):
                    arrived(h, zb, piece(p), p)
                    pass_on(h, zb, p, rising)

                each(t, one)

        loop(0, early, take)
        for h in others:
            if t == 0:
                share(h, z, 1)
            else:
                each(t, lambda zb, rising, h=h: share(h, zb, 1))

    for k in range(nz):
        for j in range(1, nx):
            send_tokens(j, nearest(k), 0).start()
    for k in range(nz):
        for j in range(1, nx):
            send_tokens(j, nearest(k), 1).start()
    for load in loads:
        load.wait()
    loop(0, early, lambda p: [side_early(k, p).start() for k in range(1, ny)] and None)
    loop(early, pieces, lambda p: both_ways(y, z, p))
    for k in range(1, ny):
        side(k, z, late_rows).start()
    share(y, z, 0)
    share(y, z, 1)

    for start in range(0, length, 128):
        row = gate_ref[:, start : start + 128]
        gcol[start : start + 128, :] = jnp.broadcast_to(row, (128, 128)).T
    acc[...] = jnp.zeros_like(acc)
    own_load.wait()

    def add(h, zb, i, part):
        weights = wbuf[h, pl.ds(zb * cores, cores)].reshape(chunk, 3 * head)
        acc[h, i, part, :] += jnp.dot(
            xbuf[i, part, columns(zb)], weights, preferred_element_type=jnp.float32
        )

    everything = pl.ds(0, tok)

    def add_others(k):
        zb = nearest(k)
        for h in others:
            arrived(h, zb, late_rows, early)
            share(h, zb, 0)
        for h in others:
            shared(h, zb)
            add(h, zb, x, everything)
        tokens_here(zb, 0)
        for h in others:
            for j in range(1, nx):
                add(h, zb, (x + j) % nx, parts[0])

    def add_last_rows(k):
        zb = nearest(k)
        tokens_here(zb, 1)
        for h in others:
            for j in range(1, nx):
                add(h, zb, (x + j) % nx, parts[1])

    def add_own(k):
        zb = nearest(k)
        if k > 0:

            @pl.when(jnp.logical_not(inner))
            def _():
                loop(0, early, lambda p: arrived(y, zb, piece(p), p))
                share(y, zb, 1)

        shared(y, zb)
        for i in range(nx):
            add(y, zb, i, everything)

    def own_rows(i, g):
        at = y * group + i * tok + (split if g else 0)
        return pl.ds(pl.multiple_of(at, 16), parts[g].size)

    def send_qkv(k, i, g):
        return pltpu.make_async_remote_copy(
            src_ref=qout.at[k - 1, i, parts[g]], dst_ref=qkv.at[own_rows(i, g)],
            send_sem=qsend.at[k - 1, i, g], recv_sem=qrecv.at[y, i, g],
            device_id=aside(k), device_id_type=MESH,
        )

    def swap(i, g):
        for k in range(1, ny):
            qout[k - 1, i, parts[g], :] = acc[others[k - 1], i, parts[g], :].astype(jnp.bfloat16)
            send_qkv(k, i, g).start()

    for t in range(1, nz):
        relay_own(t, True)
        relay_other(t - 1)
        if t == 1:

            @pl.when(jnp.logical_not(inner))
            def _():
                loop(0, early, lambda p: both_ways(y, z, p))

        if t > 1:
            add_others(t - 2)
    relay_other(nz - 1)

    @pl.when(inner)
    def _():
        loop(0, early, lambda p: both_ways(y, z, p))
        relay_own(1, False)

    for k in range(max(nz - 2, 0), nz):
        add_others(k)
    for g in range(2):
        swap(x, g)
    for j in range(1, nx):
        swap((x + j) % nx, 0)

    @pl.when(inner)
    def _():
        for t in range(2, nz):
            relay_own(t, False)

    add_last_rows(0)
    add_own(0)
    if nz > 1:
        add_last_rows(1)
        add_own(1)
    for k in range(2, nz):
        add_last_rows(k)
    for j in range(1, nx):
        swap((x + j) % nx, 1)
    for k in range(2, nz):
        add_own(k)
    for i in range(nx):
        for g in range(2):
            qkv[own_rows(i, g), :] = acc[y, i, parts[g], :].astype(jnp.bfloat16)
    for k in range(1, ny):
        other = (y + k) % ny
        for i in range(nx):
            for g in range(2):
                at = other * group + i * tok + (split if g else 0)
                taken = pl.ds(pl.multiple_of(at, 16), parts[g].size)
                pltpu.make_async_remote_copy(
                    src_ref=qout.at[k - 1, i, parts[g]], dst_ref=qkv.at[taken],
                    send_sem=qsend.at[k - 1, i, g], recv_sem=qrecv.at[other, i, g],
                    device_id={"sp": other * nx + x}, device_id_type=MESH,
                ).wait_recv()

    def send_out(to):
        return pltpu.make_async_remote_copy(
            src_ref=attn.at[pl.ds(to * tok, tok)],
            dst_ref=obuf.at[:, pl.ds(pl.multiple_of(s * head, head), head)],
            send_sem=osend.at[to], recv_sem=orecv.at[s],
            device_id={"sp": to}, device_id_type=MESH,
        )

    scale = head ** (-0.5)
    sent = 0
    for start in range(0, length, block_rows):
        finish = min(start + block_rows, length)
        scores = (
            lax.dot_general(
                qkv[start:finish, :head], qkv[:finish, head : 2 * head],
                (((1,), (1,)), ((), ())), preferred_element_type=jnp.float32,
            )
            * scale
        )
        scores = scores + gcol[start:finish, :1] - gate_ref[:, :finish]
        rows_at = start + lax.broadcasted_iota(jnp.int32, scores.shape, 0)
        cols_at = lax.broadcasted_iota(jnp.int32, scores.shape, 1)
        scores = jnp.where(cols_at <= rows_at, scores, -1e30)
        top = jnp.max(scores, axis=1, keepdims=True)
        weights = jnp.exp(scores - top)
        total = jnp.sum(weights, axis=1, keepdims=True)
        summed = jnp.dot(
            weights.astype(jnp.bfloat16), qkv[:finish, 2 * head :],
            preferred_element_type=jnp.float32,
        )
        attn[start:finish, :] = (summed / total).astype(jnp.bfloat16)
        while (sent + 1) * tok <= finish:

            @pl.when(s != sent)
            def _(to=sent):
                send_out(to).start()

            @pl.when(s == sent)
            def _(to=sent):
                obuf[:, pl.ds(pl.multiple_of(s * head, head), head)] = attn[
                    to * tok : (to + 1) * tok, :
                ]

            sent += 1

    for k in range(1, nx * ny):
        source = (s + k) % (nx * ny)
        pltpu.make_async_remote_copy(
            src_ref=attn.at[pl.ds(0, tok)],
            dst_ref=obuf.at[:, pl.ds(pl.multiple_of(source * head, head), head)],
            send_sem=osend.at[source], recv_sem=orecv.at[source],
            device_id={"sp": source}, device_id_type=MESH,
        ).wait_recv()
    last = pltpu.make_async_copy(obuf, out_ref, lsem.at[0])
    last.start()

    for zb in range(nz):
        for j in range(1, nx):
            for g in range(2):
                send_tokens(j, zb, g).wait_send()
        upward = (z < nz - 1) & (zb <= z)
        downward = (z > 0) & (zb >= z)
        whole = pl.ds(0, rows)
        for h, part in [(y, whole)] + [(h, early_rows) for h in others]:
            pl.when(upward)(lambda: up(h, zb, part, 0).wait_send())
            pl.when(downward)(lambda: down(h, zb, part, 0).wait_send())
            if cores > 1:
                for which in range(2):
                    pair(h, zb, which, c).wait_send()
        for k in range(1, ny):
            side(k, zb, late_rows).wait_send()
    for k in range(1, ny):
        copy_block(y, d, early_rows, sideq.at[k - 1], wrecv.at[y, z, 0], aside(k)).wait_send()
    for k in range(1, ny):
        for i in range(nx):
            for g in range(2):
                send_qkv(k, i, g).wait_send()
    for to in range(nx * ny):
        pl.when(s != to)(lambda to=to: send_out(to).wait_send())
    last.wait()


def body(sp, dp, tokens, query_weight, key_weight, value_weight, cum_gate):
    nx = max(n for n in range(1, math.isqrt(sp) + 1) if sp % n == 0)
    ny = sp // nx
    cores = 2 if dp % 2 == 0 else 1
    nz = dp // cores
    tok, depth = tokens.shape[1:]
    rows, head = query_weight.shape
    length = sp * tok
    split = tok * 3 // 4 // 16 * 16
    sub = min(64, rows // 4)
    early = max(rows // sub * 3 // 8, 1)
    dma = pltpu.SemaphoreType.DMA
    anywhere = pl.BlockSpec(memory_space=pl.ANY)
    vmem = pl.BlockSpec(memory_space=pltpu.VMEM)
    out = pl.pallas_call(
        functools.partial(kernel, nx, ny, nz, cores, split, sub, early),
        out_shape=jax.ShapeDtypeStruct((tok, sp * head), jnp.bfloat16),
        in_specs=[anywhere] * 4 + [vmem],
        out_specs=anywhere,
        scratch_shapes=[
            pltpu.VMEM((nx, tok, depth), jnp.bfloat16),
            pltpu.VMEM((ny, dp, rows, 3 * head), jnp.bfloat16),
            pltpu.VMEM((ny, nx, tok, 3 * head), jnp.float32),
            pltpu.VMEM((length, 3 * head), jnp.bfloat16),
            pltpu.VMEM((ny - 1, nx, tok, 3 * head), jnp.bfloat16),
            pltpu.VMEM((length, 128), jnp.float32),
            pltpu.VMEM((length, head), jnp.bfloat16),
            pltpu.VMEM((tok, sp * head), jnp.bfloat16),
            dma((3,)),
            dma,
            dma((nx - 1, nz, 2)),
            dma((nx, nz, 2)),
            dma((ny, nz, rows // sub)),
            dma((ny, nz, 2)),
            dma((ny, nz)),
            dma((ny, nz)),
            dma((ny - 1,)),
            dma((ny - 1, nz)),
            dma((ny, nz, 2)),
            dma((ny - 1, nx, 2)),
            dma((ny, nx, 2)),
            dma((sp,)),
            dma((sp,)),
        ],
        compiler_params=pltpu.CompilerParams(
            collective_id=0, has_side_effects=True, vmem_limit_bytes=60 * 1024 * 1024
        ),
    )(tokens[0], query_weight, key_weight, value_weight, cum_gate[0])
    return out[None]


def solution(mesh):
    in_specs = (
        P("dp", "sp", None),
        P("dp", "sp"),
        P("dp", "sp"),
        P("dp", "sp"),
        P("dp", "sp", None),
    )
    out_specs = P("dp", "sp", None)
    return jax.shard_map(
        functools.partial(body, mesh.shape["sp"], mesh.shape["dp"]),
        mesh=mesh, in_specs=in_specs, out_specs=out_specs, check_vma=False,
    )
```

time: 59 us -> 52.6 us (0.89)
  Pallas kernels: 57.2 us -> 50.9 us
    pallas_call x1, Pallas kernels: 57.2 us -> 50.9 us  [body(): pl.pallas_call(functools.partial(kernel, nx, ny, nz, cores, split, sub, e...]
where the time goes in v1:
time: 52.6 us; the launch traced here: 52.5 us
  Pallas kernels  50.9 us (97%)
  local copies, waits for them, and re-layouts  1.62 us (3%)
    pallas_call x1, Pallas kernels, body(): pl.pallas_call(functools.partial(kernel, nx, ny, nz, cores, split, sub, e...  50.9 us
    unnamed x1, local copies, waits for them, and re-layouts  1.62 us

profile of v1, /device:TPU:0, one launch (start us, length us, event | category | flops | bytes accessed | tf_op | source)
XLA Modules:
  0.0 52.5 jit_solution(15712969810526202099)
XLA Ops:
  0.0 50.9 %shard_map.55 = bf16[192,512]{1,0:T(8,128)(2,1)} custom-call(bf16[192,4096]{1,0:T(8,128)(2,1)} %bitcast.3, bf16[512,128]{1,0:T(8,128)(2,1)} %wq_hbm.1, bf16[512,128]{1,0:T(8,128)(2,1)} %wk_hbm.1, bf16[512,128]{1,0:T(8,128)(2,1)} %wv_hbm.1, f32[1,768]{1,0:T(1,128)} %bitcast.5), custom_call_target="tpu_custom_call" | custom-call | tf_op jit(solution)/shard_map/pallas_call | solution.py:431
  50.9 1.6 %copy.7 = bf16[1,192,512]{2,1,0:T(8,128)(2,1)} copy(bf16[1,192,512]{2,1,0:T(8,128)(2,1)} %bitcast.4) | data formatting | bytes 393216
